TPU v7x, 32 devices: a whole 2x2x4 slice. The times are simulated.
32 devices in a mesh: ep: 8 (over z, core), tp: 4 (over y, x).
Axes of the slice: x: 2, y: 2, z: 4, core: 2. Of those that a mesh axis runs over, the one named last changes fastest.
Arguments:
- queries: bfloat16 [1024, 4096], P('ep', 'tp'), may hold values from -32 to 32
- keys: bfloat16 [1024, 2048], P('ep', 'tp'), may hold values from -32 to 32
- values: bfloat16 [1024, 2048], P('ep', 'tp'), may hold values from -6 to 6
- query_gain: float32 [128], replicated, may hold values from 1 to 6
- key_gain: float32 [128], replicated, may hold values from 1 to 6
- out_weight: bfloat16 [4096, 2048], P('tp'), may hold values from -0.75 to 0.75
- expert_input: bfloat16 [1024, 2048], P('ep'), may hold values from -64 to 64
- norm_gain: float32 [2048], replicated, may hold values from 0.1 to 1.9
- routes: int32 [1024, 2], P('ep'), may hold values from 0 to 7, all different within a row; in each aligned block of 128 rows (0 to 127, 128 to 255, ...) at most 40 rows name the same one
- route_logits: float32 [1024, 2], P('ep'), may hold values from -6 to 6
- gate_weight: bfloat16 [8, 2048, 2816], P('ep', None, 'tp'), may hold values from -0.125 to 0.125
- up_weight: bfloat16 [8, 2048, 2816], P('ep', None, 'tp'), may hold values from -0.125 to 0.125
- down_weight: bfloat16 [8, 2816, 2048], P('ep', 'tp'), may hold values from -0.109375 to 0.109375
Outputs:
- mixed: bfloat16 [1024, 2048], P(('ep', 'tp'))
- expert_out: bfloat16 [1024, 2048], P('ep', 'tp')
Inputs may be any that keep to these rules, and one draw needn't show every extreme that they name: `routes`: A token's 2 experts differ. Among the 128 tokens of one index of ep (aligned blocks), no expert is named by more than 40 tokens, a bound that some block reaches.
All inputs are finite; a program needn't handle non-finite values.
Results may differ from a plain program's by a relative error of at most 0.015.
The roundings to bfloat16 on the way count: a program that leaves them out, or rounds other values in their place, can miss the bound.
Values may be sent and summed in bfloat16 or wider, within the bound.
No kernel may reach another device: no remote copies, remote signals or barrier semaphores. Data moves between devices by JAX's collectives and lax.ppermute only.
A program may use at most 64 MiB of HBM per device.

v0:
```python
import jax
import jax.numpy as jnp
from jax import lax
from jax.sharding import PartitionSpec as P

GRID_W = 64


def rope_tables(count, offset, head_dim):
    pos = offset + lax.iota(jnp.int32, count)
    grid_row = (pos // GRID_W).astype(jnp.float32)
    grid_col = (pos % GRID_W).astype(jnp.float32)
    quarter = head_dim // 4
    inverse = 10000.0 ** (-jnp.arange(quarter, dtype=jnp.float32) / quarter)
    angles = jnp.concatenate([grid_row[:, None] * inverse, grid_col[:, None] * inverse], axis=-1)
    return (jnp.cos(angles), jnp.sin(angles))


def norm_rotate(x, gain, cosine, sine):
    count, number, head_dim = x.shape
    y = x * lax.rsqrt(jnp.mean(x * x, axis=-1, keepdims=True) + 1e-06) * gain
    pairs = y.reshape(count, number, head_dim // 2, 2)
    first, second = (pairs[..., 0], pairs[..., 1])
    cos_b = cosine[:, None, :]
    sin_b = sine[:, None, :]
    turned = jnp.stack([first * cos_b - second * sin_b, first * sin_b + second * cos_b], axis=-1)
    return turned.reshape(count, number, head_dim).astype(jnp.bfloat16)


def key_block_size(length, shard_rows):
    if length <= 2048:
        return length
    shards = length // shard_rows
    most = max(1, 2048 // shard_rows)
    best = 1
    for count in range(1, most + 1):
        if shards % count == 0:
            best = count
    return best * shard_rows


def local(
    queries,
    keys,
    values,
    query_gain,
    key_gain,
    out_weight,
    expert_input,
    norm_gain,
    routes,
    route_logits,
    gate_weight,
    up_weight,
    down_weight,
):
    tokens_here = queries.shape[0]
    head_dim = query_gain.shape[0]
    heads_here = queries.shape[1] // head_dim
    kv_here = keys.shape[1] // head_dim
    group = heads_here // kv_here
    offset = lax.axis_index("ep") * tokens_here
    cosine, sine = rope_tables(tokens_here, offset, head_dim)
    q_rot = norm_rotate(
        queries.astype(jnp.float32).reshape(tokens_here, heads_here, head_dim),
        query_gain,
        cosine,
        sine,
    )
    k_rot = norm_rotate(
        keys.astype(jnp.float32).reshape(tokens_here, kv_here, head_dim), key_gain, cosine, sine
    ).reshape(tokens_here, kv_here * head_dim)
    q_grouped = q_rot.reshape(tokens_here, kv_here, group, head_dim).transpose(1, 2, 0, 3)
    q_grouped = q_grouped.reshape(kv_here, group * tokens_here, head_dim)
    query_rows = group * tokens_here
    scale = head_dim ** (-0.5)
    start_state = (
        jnp.full((kv_here, query_rows), -1e30, jnp.float32),
        jnp.zeros((kv_here, query_rows), jnp.float32),
        jnp.zeros((kv_here, query_rows, head_dim), jnp.float32),
    )
    key_piece = lax.all_gather(k_rot, "ep", axis=0, tiled=True)
    value_piece = lax.all_gather(values, "ep", axis=0, tiled=True)
    length = key_piece.shape[0]
    block = key_block_size(length, tokens_here)
    key_blocks = key_piece.reshape(length // block, block, kv_here, head_dim)
    value_blocks = value_piece.reshape(length // block, block, kv_here, head_dim)

    def step(state, blocks):
        running_max, running_total, running_sum = state
        key_block, value_block = blocks
        scores = (
            jnp.einsum("kqd,lkd->kql", q_grouped, key_block, preferred_element_type=jnp.float32)
            * scale
        )
        new_max = jnp.maximum(running_max, jnp.max(scores, axis=-1))
        factor = jnp.exp(running_max - new_max)
        weights = jnp.exp(scores - new_max[..., None])
        new_total = running_total * factor + jnp.sum(weights, axis=-1)
        new_sum = running_sum * factor[..., None] + jnp.einsum(
            "kql,lkd->kqd",
            weights.astype(jnp.bfloat16),
            value_block,
            preferred_element_type=jnp.float32,
        )
        return ((new_max, new_total, new_sum), None)

    result, _ = lax.scan(step, start_state, (key_blocks, value_blocks))
    final_max, final_total, final_sum = result
    attended = (final_sum / final_total[..., None]).astype(jnp.bfloat16)
    attended = attended.reshape(kv_here, group, tokens_here, head_dim).transpose(2, 0, 1, 3)
    attended = attended.reshape(tokens_here, heads_here * head_dim)
    summed = lax.psum_scatter(
        jnp.dot(attended, out_weight, preferred_element_type=jnp.float32).astype(jnp.bfloat16),
        "tp",
        scatter_dimension=0,
        tiled=True,
    ).astype(jnp.float32)
    mixed = summed.astype(jnp.bfloat16)
    expert_tokens_here, width = expert_input.shape
    n_ep = lax.axis_size("ep")
    top = routes.shape[1]
    capacity = expert_tokens_here * top // n_ep * 5 // 4
    x = expert_input.astype(jnp.float32)
    normed = (x * lax.rsqrt(jnp.mean(x * x, axis=-1, keepdims=True) + 1e-06) * norm_gain).astype(
        jnp.bfloat16
    )
    expert_ids = routes.reshape(-1)
    onehot = (expert_ids[:, None] == lax.iota(jnp.int32, n_ep)[None, :]).astype(jnp.int32)
    before = jnp.cumsum(onehot, axis=0) - onehot
    slot = jnp.sum(before * onehot, axis=1)
    target = expert_ids * capacity + slot
    owner_row = lax.iota(jnp.int32, expert_tokens_here * top) // top
    w_gate = gate_weight[0]
    w_up = up_weight[0]
    w_down = down_weight[0]
    columns = normed.shape[1]
    filled = jnp.zeros((n_ep * capacity, columns), jnp.bfloat16).at[target].set(normed[owner_row])
    arrived = lax.all_to_all(
        filled.reshape(n_ep, capacity, columns), "ep", split_axis=0, concat_axis=0, tiled=True
    )
    sources, slots, work_columns = arrived.shape
    flat = arrived.reshape(sources * slots, work_columns)
    gate = jnp.dot(flat, w_gate, preferred_element_type=jnp.float32)
    upper = jnp.dot(flat, w_up, preferred_element_type=jnp.float32)
    hidden = (jax.nn.silu(gate) * upper).astype(jnp.bfloat16)
    partial_out = jnp.dot(hidden, w_down, preferred_element_type=jnp.float32)
    summed = lax.psum_scatter(
        partial_out.reshape(sources, slots, width).astype(jnp.bfloat16),
        "tp",
        scatter_dimension=2,
        tiled=True,
    ).astype(jnp.float32)
    returned = lax.all_to_all(
        summed.astype(jnp.bfloat16), "ep", split_axis=0, concat_axis=0, tiled=True
    )
    picked = returned.reshape(n_ep * capacity, -1)[target].reshape(expert_tokens_here, top, -1)
    route_weight = jax.nn.sigmoid(route_logits - route_logits[:, ::-1])
    combined = jnp.sum(route_weight[..., None] * picked.astype(jnp.float32), axis=1)
    expert_out = combined.astype(jnp.bfloat16)
    return (mixed, expert_out)


def solution(mesh):
    placed = (
        P("ep", "tp"),
        P("ep", "tp"),
        P("ep", "tp"),
        P(),
        P(),
        P("tp", None),
        P("ep", None),
        P(),
        P("ep", None),
        P("ep", None),
        P("ep", None, "tp"),
        P("ep", None, "tp"),
        P("ep", "tp", None),
    )
    return jax.shard_map(
        local,
        mesh=mesh,
        in_specs=placed,
        out_specs=(P(("ep", "tp"), None), P("ep", "tp")),
        check_vma=False,
    )
```

profile of v0, /device:TPU:0, one launch (start us, length us, event | category | flops | bytes accessed | tf_op | source)
XLA Modules:
  0.0 149.4 jit_solution(6577573726553439491)
XLA Ops:
  9.2 1.0 copy.19
  10.3 1.4 mul.250
  12.6 0.9 multiply_multiply_fusion.1
  13.9 0.9 pad_maximum_fusion.1
  19.5 1.3 fusion.24
  22.2 1.0 fusion.26
  23.2 6.8 %scatter_custom_fusion = bf16[320,2048]{1,0:T(8,128)(2,1)} fusion(s32[256]{0:T(256)S(1)} %bitcast.68, bf16[128,2048]{1,0:T(8,128)(2,1)} %fusion.26, s32[1024]{0:T(1024)S(1)} %pad_clamp_fusion.1, bf16[]{:T(256)} %constant.100.clone.1), kind=kCustom, calls=%fused_computation.26 | custom fusion | bytes 1311232 | tf_op jit(solution)/shard_map/scatter | solution.py:138
  30.0 6.3 %all-to-all-start = ((bf16[8,40,2048]{2,1,0:T(8,128)(2,1)}), bf16[8,40,2048]{2,1,0:T(8,128)(2,1)}, u32[]{:S(2)}, u32[]{:S(2)}) async-start(bf16[8,40,2048]{2,1,0:T(8,128)(2,1)} %bitcast.59), calls=%async_computation.1 | async-start | bytes 2621440 | tf_op jit(solution)/shard_map/all_to_all | solution.py:139
  37.4 39.6 %all-to-all-done = bf16[8,40,2048]{2,1,0:T(8,128)(2,1)} async-done(((bf16[8,40,2048]{2,1,0:T(8,128)(2,1)}), bf16[8,40,2048]{2,1,0:T(8,128)(2,1)}, u32[]{:S(2)}, u32[]{:S(2)}) %all-to-all-start) | async-done | bytes 1310752 | tf_op jit(solution)/shard_map/all_to_all | solution.py:139
  77.0 3.6 %fusion.6 = f32[320,704]{1,0:T(8,128)S(1)} fusion(bf16[320,2048]{1,0:T(8,128)(2,1)} %bitcast.19, bf16[1,2048,704]{1,2,0:T(8,128)(2,1)} %param.23), kind=kOutput, calls=%fused_computation.11 | convolution fusion | flops 922746880 | bytes 5095424 | tf_op jit(solution)/shard_map/dot_general | solution.py:144
  80.6 2.6 %fusion.18 = bf16[320,704]{1,0:T(8,128)(2,1)S(1)} fusion(bf16[320,2048]{1,0:T(8,128)(2,1)} %bitcast.19, bf16[1,2048,704]{1,2,0:T(8,128)(2,1)S(1)} %copy-done.12, f32[320,704]{1,0:T(8,128)S(1)} %fusion.6), kind=kOutput, calls=%fused_computation.21 | convolution fusion | flops 924098560 | bytes 5545984 | tf_op jit(solution)/shard_map/dot_general | solution.py:145
  83.2 2.3 %fusion.8 = bf16[8,40,2048]{2,1,0:T(8,128)(2,1)} fusion(bf16[8,40,704]{2,1,0:T(8,128)(2,1)S(1)} %bitcast.73, bf16[1,704,2048]{2,1,0:T(8,128)(2,1)S(1)} %copy-done), kind=kOutput, calls=%fused_computation.13 | convolution fusion | flops 923402240 | bytes 4644864 | tf_op jit(solution)/shard_map/dot_general | solution.py:147
  87.7 2.0 %multiply_reduce_fusion = (f32[4,256]{1,0:T(4,128)S(1)}, f32[4,256,1024]{2,1,0:T(8,128)S(1)}) fusion(bf16[4,256,128]{2,1,0:T(8,128)(2,1)S(1)} %bitcast.62, bf16[1024,4,128]{0,2,1:T(8,128)(2,1)} %bitcast.65), kind=kOutput, calls=%fused_computation.4 | convolution fusion | flops 270531584 | bytes 5509120 | tf_op jit(solution)/shard_map/while/body/eval_jaxpr/kqd,lkd->kql/dot_general | solution.py:93
  89.7 1.9 %copy-done.1 = f32[4,256,1024]{2,1,0:T(8,128)} copy-done((f32[4,256,1024]{2,1,0:T(8,128)}, f32[4,256,1024]{2,1,0:T(8,128)S(1)}, u32[]{:S(2)}) %copy-start.1) | copy-done | bytes 4194328
  91.7 0.9 fusion
  92.6 3.5 %fusion.32 = bf16[4,256,128]{2,1,0:T(8,128)(2,1)S(1)} fusion(bf16[1024,4,128]{0,2,1:T(8,128)(2,1)} %bitcast.72, f32[4,256,1024]{2,1,0:T(8,128)} %copy-done.1, f32[4,256]{1,0:T(4,128)S(1)} %broadcast_maximum_fusion, f32[4,256]{1,0:T(4,128)S(1)} %get-tuple-element.30, f32[4,256]{1,0:T(4,128)S(1)} %get-tuple-element.29), kind=kOutput, calls=%fused_computation.29 | convolution fusion | flops 271974400 | bytes 5517312 | tf_op jit(solution)/shard_map/while/body/eval_jaxpr/kql,lkd->kqd/dot_general | solution.py:100
  96.3 3.9 %convolution_convert_fusion = bf16[128,2048]{1,0:T(8,128)(2,1)} fusion(bf16[128,1024]{0,1:T(8,128)(2,1)S(1)} %bitcast.64, bf16[1024,2048]{1,0:T(8,128)(2,1)} %param.18), kind=kOutput, calls=%fused_computation.14 | convolution fusion | flops 537133056 | bytes 4980736 | tf_op jit(solution)/shard_map/dot_general | solution.py:114
  100.2 13.4 %reduce-scatter.5.cloned.1.call-done = bf16[8,40,512]{2,1,0:T(8,128)(2,1)} async-done(((bf16[8,40,2048]{2,1,0:T(8,128)(2,1)}), bf16[8,40,512]{2,1,0:T(8,128)(2,1)}) %reduce-scatter.5.cloned.1.call-update) | async-done | bytes 327696 | tf_op jit(solution)/shard_map/reduce_scatter | solution.py:148
  113.6 4.6 %all-to-all-start.1 = ((bf16[8,40,512]{2,1,0:T(8,128)(2,1)}), bf16[8,40,512]{2,1,0:T(8,128)(2,1)S(1)}, u32[]{:S(2)}, u32[]{:S(2)}) async-start(bf16[8,40,512]{2,1,0:T(8,128)(2,1)} %reduce-scatter.5.cloned.1.call-done), calls=%async_computation.3 | async-start | bytes 655360 | tf_op jit(solution)/shard_map/all_to_all | solution.py:154
  118.4 10.9 %all-to-all-done.1 = bf16[8,40,512]{2,1,0:T(8,128)(2,1)S(1)} async-done(((bf16[8,40,512]{2,1,0:T(8,128)(2,1)}), bf16[8,40,512]{2,1,0:T(8,128)(2,1)S(1)}, u32[]{:S(2)}, u32[]{:S(2)}) %all-to-all-start.1) | async-done | bytes 327712 | tf_op jit(solution)/shard_map/all_to_all | solution.py:154
  129.4 1.9 %gather_fusion = bf16[256,512]{1,0:T(8,128)(2,1)} fusion(bf16[320,512]{1,0:T(8,128)(2,1)S(1)} %bitcast.58, s32[1024]{0:T(1024)S(1)} %pad_clamp_fusion), kind=kCustom, calls=%fused_computation.1 | custom fusion | bytes 525312 | tf_op jit(solution)/shard_map/gather | solution.py:157
  131.2 1.3 reshape.288
  132.5 1.4 multiply_reduce_fusion.1
  133.9 8.1 %reduce-scatter.3.cloned.1.call-done = bf16[32,2048]{1,0:T(8,128)(2,1)} async-done(((bf16[128,2048]{1,0:T(8,128)(2,1)}), bf16[32,2048]{1,0:T(8,128)(2,1)}) %reduce-scatter.3.cloned.1.call-update) | async-done | bytes 131088 | tf_op jit(solution)/shard_map/reduce_scatter | solution.py:113
  (74 shorter events, 12.2 us)
Async XLA Ops:
  8.0 75.2 %copy-start = (bf16[1,704,2048]{2,1,0:T(8,128)(2,1)S(1)}, bf16[1,704,2048]{2,1,0:T(8,128)(2,1)}, u32[]{:S(2)}) copy-start(bf16[1,704,2048]{2,1,0:T(8,128)(2,1)} %param.25) | copy-start | bytes 8650756
  8.0 14.2 %copy-start.2 = (bf16[128,2048]{1,0:T(8,128)(2,1)S(1)}, bf16[128,2048]{1,0:T(8,128)(2,1)}, u32[]{:S(2)}) copy-start(bf16[128,2048]{1,0:T(8,128)(2,1)} %param.19) | copy-start | bytes 1572868
  8.0 14.2 %copy-start.9 = (f32[2048]{0:T(1024)S(1)}, f32[2048]{0:T(1024)}, u32[]{:S(2)}) copy-start(f32[2048]{0:T(1024)} %param.20) | copy-start | bytes 24580
  8.0 79.7 %all-gather.3.cloned.1.call-start = ((), (), s32[]{:S(2)}) async-start(), calls=%async_computation.4 | async-start | bytes 1179648 | tf_op jit(solution)/shard_map/all_gather | solution.py:82
  12.6 2.2 %copy-start.3 = (f32[128,64]{0,1:T(8,128)}, f32[128,64]{0,1:T(8,128)S(1)}, u32[]{:S(2)}) copy-start(f32[128,64]{0,1:T(8,128)S(1)} %get-tuple-element.20) | copy-start | bytes 98308
  12.6 2.2 %copy-start.5 = (f32[128,64]{0,1:T(8,128)}, f32[128,64]{0,1:T(8,128)S(1)}, u32[]{:S(2)}) copy-start(f32[128,64]{0,1:T(8,128)S(1)} %get-tuple-element.28) | copy-start | bytes 98308
  19.5 16.9 %copy-start.8 = (bf16[128,512]{1,0:T(8,128)(2,1)S(1)}, bf16[128,512]{1,0:T(8,128)(2,1)}, u32[]{:S(2)}) copy-start(bf16[128,512]{1,0:T(8,128)(2,1)} %param.15) | copy-start | bytes 393220
  23.2 14.0 %copy-start.7 = (bf16[128,1024]{1,0:T(8,128)(2,1)S(1)}, bf16[128,1024]{1,0:T(8,128)(2,1)}, u32[]{:S(2)}) copy-start(bf16[128,1024]{1,0:T(8,128)(2,1)} %param.13) | copy-start | bytes 786436
  30.0 47.0 %all-to-all-start = ((bf16[8,40,2048]{2,1,0:T(8,128)(2,1)}), bf16[8,40,2048]{2,1,0:T(8,128)(2,1)}, u32[]{:S(2)}, u32[]{:S(2)}) async-start(bf16[8,40,2048]{2,1,0:T(8,128)(2,1)} %bitcast.59), calls=%async_computation.1 | async-start | bytes 2621440 | tf_op jit(solution)/shard_map/all_to_all | solution.py:139
  36.3 56.3 %all-gather.5.cloned.1.call-start = ((), (), s32[]{:S(2)}) async-start(), calls=%async_computation.5 | async-start | bytes 1179648 | tf_op jit(solution)/shard_map/all_gather | solution.py:83
  37.1 76.5 %reduce-scatter.5.cloned.1.call-start = ((), (), s32[]{:S(2)}) async-start(), calls=%async_computation.7 | async-start | bytes 1638400 | tf_op jit(solution)/shard_map/reduce_scatter | solution.py:148
  77.0 3.6 %copy-start.12 = (bf16[1,2048,704]{1,2,0:T(8,128)(2,1)S(1)}, bf16[1,2048,704]{1,2,0:T(8,128)(2,1)}, u32[]{:S(2)}) copy-start(bf16[1,2048,704]{1,2,0:T(8,128)(2,1)} %param.24) | copy-start | bytes 8650756
  83.2 2.6 %copy-start.11 = (f32[128]{0:T(128)S(1)}, f32[128]{0:T(128)}, u32[]{:S(2)}) copy-start(f32[128]{0:T(128)} %param.16) | copy-start | bytes 1540
  83.2 3.0 %copy-start.4 = (f32[128,64]{0,1:T(8,128)S(1)}, f32[128,64]{0,1:T(8,128)}, u32[]{:S(2)}) copy-start(f32[128,64]{0,1:T(8,128)} %copy-done.3) | copy-start | bytes 98308
  83.2 3.0 %copy-start.6 = (f32[128,64]{0,1:T(8,128)S(1)}, f32[128,64]{0,1:T(8,128)}, u32[]{:S(2)}) copy-start(f32[128,64]{0,1:T(8,128)} %copy-done.5) | copy-start | bytes 98308
  85.5 56.4 %reduce-scatter.3.cloned.1.call-start = ((), (), s32[]{:S(2)}) async-start(), calls=%async_computation.6 | async-start | bytes 655360 | tf_op jit(solution)/shard_map/reduce_scatter | solution.py:113
  89.7 1.9 %copy-start.1 = (f32[4,256,1024]{2,1,0:T(8,128)}, f32[4,256,1024]{2,1,0:T(8,128)S(1)}, u32[]{:S(2)}) copy-start(f32[4,256,1024]{2,1,0:T(8,128)S(1)} %get-tuple-element.34) | copy-start | bytes 12582916
  96.3 22.0 %copy-start.10 = (f32[128,2]{0,1:T(2,128)S(1)}, f32[128,2]{0,1:T(2,128)}, u32[]{:S(2)}) copy-start(f32[128,2]{0,1:T(2,128)} %param.22) | copy-start | bytes 3076
  113.6 15.7 %all-to-all-start.1 = ((bf16[8,40,512]{2,1,0:T(8,128)(2,1)}), bf16[8,40,512]{2,1,0:T(8,128)(2,1)S(1)}, u32[]{:S(2)}, u32[]{:S(2)}) async-start(bf16[8,40,512]{2,1,0:T(8,128)(2,1)} %reduce-scatter.5.cloned.1.call-done), calls=%async_computation.3 | async-start | bytes 655360 | tf_op jit(solution)/shard_map/all_to_all | solution.py:154
Sparse Core Ops, SparseCore 0:
  15.0 26.5 all-gather.2
  43.8 34.2 all-gather.4
Sparse Core Ops, SparseCore 1:
  85.6 28.0 reduce-scatter.4
  116.9 25.0 reduce-scatter.2
where the time goes:
time: 150 us; the launch traced here: 149 us
  waiting for transfers between devices  72.1 us (48%)
  local copies, waits for them, and re-layouts  19.2 us (13%)
  matrix products  17.8 us (12%)
  between operations  15.8 us (11%)
  other arithmetic  13.3 us (9%)
  starting transfers between devices  11.2 us (7%)
    all_to_all x1, waiting for transfers between devices, local(): lax.all_to_all(filled.reshape(n_ep, capacity, columns), 'ep', split_axis=...  39.6 us
    reduce_scatter x1, waiting for transfers between devices, local(): lax.psum_scatter(partial_out.reshape(sources, slots, width).astype(jnp.bf...  13.4 us
    all_to_all x1, waiting for transfers between devices, local(): lax.all_to_all(summed.astype(jnp.bfloat16), 'ep', split_axis=0, concat_ax...  10.9 us
    reduce_scatter x1, waiting for transfers between devices, local(): lax.psum_scatter(jnp.dot(attended, out_weight, preferred_element_type=jnp...  8.1 us
    scatter x1, local copies, waits for them, and re-layouts, local(): jnp.zeros((n_ep * capacity, columns), jnp.bfloat16).at[target]  6.79 us
    all_to_all x1, starting transfers between devices, local(): lax.all_to_all(filled.reshape(n_ep, capacity, columns), 'ep', split_axis=...  6.26 us
    unnamed x30, local copies, waits for them, and re-layouts  4.71 us
    all_to_all x1, starting transfers between devices, local(): lax.all_to_all(summed.astype(jnp.bfloat16), 'ep', split_axis=0, concat_ax...  4.6 us
  transfers between devices with their start and end apart: 6, of which 4 were waited for; matrix products, arithmetic and copies ran while one was open for 28% of the time, Pallas kernels for 0%

commit v1 on v0

--- a/solution.py
+++ b/solution.py
@@ -1,7 +1,16 @@
+import functools
+
 import jax
 import jax.numpy as jnp
+import numpy as np
 from jax import lax
+from jax.experimental import pallas as pl
+from jax.experimental.pallas import tpu as pltpu
 from jax.sharding import PartitionSpec as P
+
+
+F32 = jnp.float32
+BF16 = jnp.bfloat16
 
 GRID_W = 64
 
@@ -39,7 +48,7 @@
     return best * shard_rows
 
 
-def local(
+def plain_local(
     queries,
     keys,
     values,
@@ -106,7 +115,7 @@
         return ((new_max, new_total, new_sum), None)
 
     result, _ = lax.scan(step, start_state, (key_blocks, value_blocks))
-    final_max, final_total, final_sum = result
+    _, final_total, final_sum = result
     attended = (final_sum / final_total[..., None]).astype(jnp.bfloat16)
     attended = attended.reshape(kv_here, group, tokens_here, head_dim).transpose(2, 0, 1, 3)
     attended = attended.reshape(tokens_here, heads_here * head_dim)
@@ -161,6 +170,382 @@
     return (mixed, expert_out)
 
 
+def swap(x, axis, mask):
+    return lax.ppermute(x, axis, [(i, i ^ mask) for i in range(lax.axis_size(axis))])
+
+
+def spread_out(xs, axis, stride):
+    return [x if not i else swap(x, axis, stride * i) for i, x in enumerate(xs)]
+
+
+def call(body, outs, flops, moved, scratch=(), raw=0, shapes=(), kept=0):
+    vmem = pl.BlockSpec(memory_space=pltpu.VMEM)
+    hbm = pl.BlockSpec(memory_space=pl.ANY)
+    scratch = list(scratch) + [pltpu.VMEM(x.shape, x.dtype) for x in shapes]
+    if raw:
+        scratch.append(pltpu.SemaphoreType.DMA((raw,)))
+
+    def run(*args):
+        args = [pltpu.with_memory_space_constraint(x, pltpu.HBM) for x in args[:raw]] + list(args[raw:])
+        return pl.pallas_call(
+            body,
+            out_shape=[pltpu.VMEM(s, d) for s, d in outs[:kept]]
+            + [jax.ShapeDtypeStruct(s, d) for s, d in outs[kept:]],
+            in_specs=[hbm] * raw + [vmem] * (len(args) - raw),
+            out_specs=[vmem for _ in outs],
+            scratch_shapes=scratch,
+            compiler_params=pltpu.CompilerParams(vmem_limit_bytes=16 << 20),
+            cost_estimate=pl.CostEstimate(flops=flops, transcendentals=0, bytes_accessed=moved),
+        )(*args)
+
+    return run
+
+
+def fetch(sources, targets, sems):
+    copies = [
+        pltpu.make_async_copy(a, b, sems.at[i]) for i, (a, b) in enumerate(zip(sources, targets))
+    ]
+    for copy in copies:
+        copy.start()
+    return copies
+
+
+def wide(ref, offset, size):
+    return ref[:, pl.ds(pl.multiple_of(offset, 128), size)]
+
+
+def rope_body(*refs, head_dim, group, heads):
+    (q_hbm, k_hbm, v_hbm, qg_hbm, kg_hbm, inv_hbm), weights = refs[:6], refs[6:9]
+    stored, outs, loaded, sems = refs[9:12], refs[12:-7], refs[-7:-1], refs[-1]
+    copies = fetch(refs[:6] + weights, loaded + stored, sems)
+    q_ref, k_ref, v_ref, qg_ref, kg_ref, inv_ref = loaded
+    count = q_ref.shape[0]
+    me = lax.axis_index("ep")
+    side = (me // 2) & 1
+    lane = lax.broadcasted_iota(jnp.int32, (count, head_dim), 1)
+    pos = me * count + lax.broadcasted_iota(jnp.int32, (count, head_dim), 0)
+    shift = GRID_W.bit_length() - 1
+    spot = jnp.where(lane < head_dim // 2, pos >> shift, pos & (GRID_W - 1)).astype(F32)
+    for copy in copies[:6]:
+        copy.wait()
+    angle = spot * inv_ref[...]
+    even = (lane & 1) == 0
+    cosine = jnp.cos(angle)
+    sine = jnp.sin(angle)
+    sine = jnp.where(even, -sine, sine)
+
+    def turn(x, gain):
+        x = x.astype(F32)
+        y = x * lax.rsqrt(jnp.mean(x * x, axis=-1, keepdims=True) + 1e-06) * gain
+        other = jnp.where(even, pltpu.roll(y, head_dim - 1, 1), pltpu.roll(y, 1, 1))
+        return (y * cosine + other * sine).astype(BF16)
+
+    q_gain, k_gain = qg_ref[...], kg_ref[...]
+    q0, kv0, pair, kv1 = outs
+    for turned_side, q_outs, kv_outs in (
+        (side, [(q0, 0)], [(kv0, 0)]),
+        (side ^ 1, [(pair, 0)], [(pair, count), (kv1, 0)]),
+    ):
+        for h in range(heads * group):
+            x = turn(wide(q_ref, (turned_side * heads * group + h) * head_dim, head_dim), q_gain)
+            for out, row in q_outs:
+                out[row : row + count, h * head_dim : (h + 1) * head_dim] = x
+        for h in range(heads):
+            at = (turned_side * heads + h) * head_dim
+            x, v = turn(wide(k_ref, at, head_dim), k_gain), wide(v_ref, at, head_dim)
+            for out, row in kv_outs:
+                out[row : row + count, h * head_dim : (h + 1) * head_dim] = x
+                out[row : row + count, (heads + h) * head_dim : (heads + h + 1) * head_dim] = v
+    for copy in copies[6:]:
+        copy.wait()
+
+
+def attend_body(q0, q1, own, other, out0, out1, all_kv, *, head_dim, group, heads):
+    count = q0.shape[0]
+    half = own.shape[0]
+    all_kv[:half, :] = own[...]
+    all_kv[half:, :] = other[...]
+    factor = float(head_dim) ** -0.5 * float(np.log2(np.e))
+    for j in range(heads):
+        keys = all_kv[:, j * head_dim : (j + 1) * head_dim]
+        values = all_kv[:, (heads + j) * head_dim : (heads + j + 1) * head_dim]
+        for q_ref, out in ((q0, out0), (q1, out1)):
+            cols = [
+                slice(h * head_dim, (h + 1) * head_dim)
+                for h in range(j * group, (j + 1) * group)
+            ]
+            q = jnp.concatenate([q_ref[:, c] for c in cols], axis=0)
+            s = lax.dot_general(q, keys, (((1,), (1,)), ((), ())), preferred_element_type=F32)
+            top = jnp.max(s, axis=-1, keepdims=True)
+            p = jnp.exp2((s - top) * factor)
+            total = jnp.sum(p, axis=-1, keepdims=True)
+            o = jnp.dot(p.astype(BF16), values, preferred_element_type=F32)
+            o = (o / total).astype(BF16)
+            for i, c in enumerate(cols):
+                out[:, c] = o[i * count : (i + 1) * count, :]
+
+
+def project_body(*refs, splits):
+    pieces, w_ref, outs, whole = refs[:2], refs[2], refs[3 : 3 + splits], refs[3 + splits]
+    side = (lax.axis_index("ep") // 2) & 1
+    here = lax.axis_index("tp")
+    cols = pieces[0].shape[1]
+    acc = None
+    for k, piece in enumerate(pieces):
+        at = pl.multiple_of((side ^ k) * cols, cols)
+        part = jnp.dot(piece[...], w_ref[pl.ds(at, cols), :], preferred_element_type=F32)
+        acc = part if acc is None else acc + part
+    whole[...] = acc
+    rows = outs[0].shape[0]
+    for i, out in enumerate(outs):
+        out[...] = whole[pl.ds(pl.multiple_of((here ^ i) * rows, rows), rows), :].astype(BF16)
+
+
+def dispatch_body(x0_hbm, g_hbm, x1_ref, r0_ref, r1_ref, *refs, chips, capacity, experts):
+    own, sends = refs[0], refs[1:chips]
+    picks, (normed, x0_ref, g_ref, sems) = refs[chips : chips + 2], refs[chips + 2 :]
+    copies = fetch((x0_hbm, g_hbm), (x0_ref, g_ref), sems)
+    count, _ = x0_ref.shape
+    me = lax.axis_index("ep")
+    chip, core = me // 2, me & 1
+    rows = chips * 2 * capacity
+
+    def spread(shape, axis):
+        return lax.broadcasted_iota(jnp.int32, shape, axis)
+
+    ahead = (spread((count, count), 0) < spread((count, count), 1)).astype(BF16)
+    row = spread((rows, count), 0)
+    block = ((row.astype(F32) + 0.5) * (1.0 / capacity)).astype(jnp.int32)
+    slot = (row - block * capacity).astype(F32)
+    side = block & 1
+    row_e = spread((rows, experts), 0)
+    block_e = ((row_e.astype(F32) + 0.5) * (1.0 / capacity)).astype(jnp.int32)
+    target = 2 * (chip ^ (block_e >> 1)) + core
+    chooser = (target == spread((rows, experts), 1)).astype(BF16)
+    for i, ref in enumerate((r0_ref, r1_ref)):
+        named = [
+            (ref[j : j + 1, :] == spread((experts, count), 0)).astype(BF16) for j in range(2)
+        ]
+        before = jnp.dot(named[0] + named[1], ahead, preferred_element_type=F32)
+        at = jnp.dot(chooser, before.astype(BF16), preferred_element_type=F32)
+        fits = (at == slot) & (side == i)
+        for j in range(2):
+            hit = jnp.dot(chooser, named[j], preferred_element_type=F32)
+            picks[j][:, i * count : (i + 1) * count] = jnp.where(fits & (hit > 0.5), 1.0, 0.0).astype(
+                BF16
+            )
+    for copy in copies:
+        copy.wait()
+    for i, ref in enumerate((x0_ref, x1_ref)):
+        x = ref[...].astype(F32)
+        y = x * lax.rsqrt(jnp.mean(x * x, axis=-1, keepdims=True) + 1e-06) * g_ref[...]
+        normed[i * count : (i + 1) * count, :] = y.astype(BF16)
+
+    both = picks[0][...] + picks[1][...]
+    step = 2 * capacity
+    own[...] = jnp.dot(both[:step], normed[...], preferred_element_type=F32).astype(BF16)
+    part = wide(normed, lax.axis_index("tp") * sends[0].shape[1], sends[0].shape[1])
+    far = jnp.dot(both[step:], part, preferred_element_type=F32).astype(BF16)
+    for k, out in enumerate(sends):
+        out[...] = far[k * step : (k + 1) * step, :]
+
+
+def expert_body(*refs, blocks):
+    xs = refs[:blocks]
+    wg, wu, wd = refs[blocks : blocks + 3]
+    outs = refs[blocks + 3 :]
+    here = lax.axis_index("tp")
+    cols = xs[0].shape[1]
+    across = (((1,), (1,)), ((), ()))
+    gate = upper = None
+    for i, x_ref in enumerate(xs):
+        x = x_ref[...]
+        at = (here ^ i) * cols if blocks > 1 else 0
+        g = lax.dot_general(x, wide(wg, at, cols), across, preferred_element_type=F32)
+        u = lax.dot_general(x, wide(wu, at, cols), across, preferred_element_type=F32)
+        gate = g if gate is None else gate + g
+        upper = u if upper is None else upper + u
+    hidden = (jax.nn.silu(gate) * upper).astype(BF16)
+    cols = outs[0].shape[1]
+    for i, out in enumerate(outs):
+        w = wide(wd, (here ^ i) * cols, cols)
+        out[...] = jnp.dot(hidden, w, preferred_element_type=F32).astype(BF16)
+
+
+def combine_body(l0_ref, l1_ref, p0_ref, p1_ref, *refs, chips, splits):
+    homes, backs = refs[:splits], refs[splits : splits + chips - 1]
+    mine, theirs, table = refs[splits + chips - 1 :]
+    step, cols = homes[0].shape
+    total = homes[0][...].astype(F32)
+    for ref in homes[1:]:
+        total = total + ref[...].astype(F32)
+    table[:step, :] = total.astype(BF16)
+    for k, ref in enumerate(backs):
+        table[(k + 1) * step : (k + 2) * step, :] = ref[...]
+    count = l0_ref.shape[1]
+    flip = (((0,), (0,)), ((), ()))
+    picked = [
+        lax.dot_general(ref[...], table[...], flip, preferred_element_type=F32)
+        for ref in (p0_ref, p1_ref)
+    ]
+    for i, (ref, out) in enumerate(((l0_ref, mine), (l1_ref, theirs))):
+        gap = ref[0:1, :] - ref[1:2, :]
+        first = jnp.broadcast_to(jax.nn.sigmoid(gap), (count, count)).T
+        second = jnp.broadcast_to(jax.nn.sigmoid(-gap), (count, count)).T
+        rows = slice(i * count, (i + 1) * count)
+        for at in range(0, out.shape[1], count):
+            cols = slice(at, at + count)
+            out[:, cols] = first * picked[0][rows, cols] + second * picked[1][rows, cols]
+
+
+def local(
+    queries,
+    keys,
+    values,
+    query_gain,
+    key_gain,
+    out_weight,
+    expert_input,
+    norm_gain,
+    routes,
+    route_logits,
+    gate_weight,
+    up_weight,
+    down_weight,
+):
+    n_ep, n_tp = lax.axis_size("ep"), lax.axis_size("tp")
+    chips = n_ep // 2
+    count = queries.shape[0]
+    head_dim = query_gain.shape[0]
+    kv_here = keys.shape[1] // head_dim
+    group = queries.shape[1] // keys.shape[1]
+    tokens, width = expert_input.shape
+    part = width // n_tp
+    capacity = tokens * routes.shape[1] // n_ep * 5 // 4
+    step = 2 * capacity
+    rows = chips * step
+    hidden = gate_weight.shape[2]
+
+    routes, route_logits = routes.T, route_logits.T
+    x_other = swap(expert_input, "ep", 1)
+    routes_other = swap(routes, "ep", 1)
+    logits_other = swap(route_logits, "ep", 1)
+    sources = (expert_input, norm_gain.reshape(1, width))
+    made = call(
+        functools.partial(dispatch_body, chips=chips, capacity=capacity, experts=n_ep),
+        [((step, width), BF16)]
+        + [((step, part), BF16)] * (chips - 1)
+        + [((rows, 2 * tokens), BF16)] * 2,
+        2 * rows * 2 * tokens * width,
+        4 * tokens * width,
+        [pltpu.VMEM((2 * tokens, width), BF16)],
+        raw=2,
+        shapes=sources,
+    )(*sources, x_other, routes, routes_other)
+    own, picks = made[0], made[chips:]
+    arrived = spread_out(made[:chips], "ep", 2)[1:]
+    far = jnp.concatenate(arrived, axis=0)
+
+    quarter = head_dim // 4
+    inverse = (10000.0 ** (-np.arange(quarter, dtype=np.float32) / quarter)).astype(np.float32)
+    inverse = np.tile(np.repeat(inverse, 2), 2).reshape(1, head_dim)
+    heads = kv_here // 2
+    q_cols, kv_cols = heads * group * head_dim, 2 * heads * head_dim
+    gains = (query_gain.reshape(1, head_dim), key_gain.reshape(1, head_dim))
+    sources = (queries, keys, values, *gains, jnp.asarray(inverse))
+    weights = (gate_weight[0].T, up_weight[0].T, down_weight[0])
+    made = call(
+        functools.partial(rope_body, head_dim=head_dim, group=group, heads=heads),
+        [(w.shape, BF16) for w in weights]
+        + [((count, q_cols), BF16), ((count, kv_cols), BF16)]
+        + [((2 * count, kv_cols), BF16), ((count, kv_cols), BF16)],
+        count * queries.shape[1] * 60,
+        4 * count * queries.shape[1] + 6 * width * hidden,
+        raw=9,
+        shapes=sources,
+        kept=3,
+    )(*sources, *weights)
+    weights, (q0, kv0, pair, kv1) = made[:3], made[3:]
+    pair = swap(pair, "ep", 2)
+    blocks = [kv0, pair[count:]]
+    blocks += [swap((kv0, kv1)[k & 1], "ep", 2 * k) for k in range(2, chips)]
+
+    def expert(xs):
+        number = xs[0].shape[0]
+        return call(
+            functools.partial(expert_body, blocks=len(xs)),
+            [((number, part), BF16)] * n_tp,
+            6 * number * width * hidden,
+            6 * width * hidden,
+        )(*xs, *weights)
+
+    def add_up(xs):
+        total = xs[0].astype(F32)
+        for x in xs[1:]:
+            total = total + x.astype(F32)
+        return total.astype(BF16)
+
+    home = spread_out(expert([own]), "tp", 1)
+    gathered = spread_out([far] * n_tp, "tp", 1)
+
+    kv_own = jnp.concatenate(blocks, axis=0)
+    out0, out1 = call(
+        functools.partial(attend_body, head_dim=head_dim, group=group, heads=heads),
+        [((count, q_cols), BF16)] * 2,
+        8 * count * q_cols * n_ep * count,
+        8 * n_ep * count * kv_cols,
+        [pltpu.VMEM((n_ep * count, kv_cols), BF16)],
+    )(q0, pair[:count], kv_own, swap(kv_own, "ep", 1))
+    attended = (out0, swap(out1, "ep", 2))
+
+    remote = add_up(spread_out(expert(gathered), "tp", 1))
+    backs = [remote] + [remote[k * step : (k + 1) * step] for k in range(chips - 1)]
+    backs = spread_out(backs, "ep", 2)[1:]
+
+    mixed = call(
+        functools.partial(project_body, splits=n_tp),
+        [((count // n_tp, width), BF16)] * n_tp,
+        2 * count * out_weight.shape[0] * width,
+        2 * out_weight.shape[0] * width,
+        [pltpu.VMEM((count, width), F32)],
+    )(*attended, out_weight)
+    mixed = add_up(spread_out(mixed, "tp", 1))
+
+    mine, theirs = call(
+        functools.partial(combine_body, chips=chips, splits=n_tp),
+        [((tokens, part), F32)] * 2,
+        4 * rows * 2 * tokens * part,
+        4 * rows * part,
+        [pltpu.VMEM((rows, part), BF16)],
+    )(route_logits, logits_other, *picks, *home, *backs)
+    expert_out = (mine + swap(theirs, "ep", 1)).astype(BF16)
+    return (mixed, expert_out)
+
+
+def power_of_two(x):
+    return x & (x - 1) == 0
+
+
+def suits(mesh, shapes):
+    n_ep, n_tp = mesh.shape["ep"], mesh.shape["tp"]
+    queries, keys, gain, x, routes = shapes
+    if n_ep < 4 or not (power_of_two(n_ep) and power_of_two(n_tp)):
+        return False
+    count, head_dim = queries[0] // n_ep, gain[0]
+    tokens = x[0] // n_ep
+    capacity = tokens * routes[1] // n_ep * 5 // 4
+    return (
+        head_dim % 128 == 0
+        and keys[1] // n_tp % (2 * head_dim) == 0
+        and queries[1] == 2 * keys[1]
+        and count % (16 * n_tp) == 0
+        and tokens % 128 == 0
+        and capacity % 8 == 0
+        and x[1] % (128 * n_tp) == 0
+        and routes[1] == 2
+    )
+
+
 def solution(mesh):
     placed = (
         P("ep", "tp"),
@@ -177,10 +562,19 @@
         P("ep", None, "tp"),
         P("ep", "tp", None),
     )
-    return jax.shard_map(
-        local,
+
+    sharded = functools.partial(
+        jax.shard_map,
         mesh=mesh,
         in_specs=placed,
         out_specs=(P(("ep", "tp"), None), P("ep", "tp")),
         check_vma=False,
     )
+
+    def run(*args):
+        shapes = [args[j].shape for j in (0, 1, 3, 6, 8)]
+        if not suits(mesh, shapes):
+            return sharded(plain_local)(*args)
+        return sharded(local)(*args)
+
+    return run

time: 150 us -> 82 us (0.55)
  waiting for transfers between devices: 72.1 us -> 29.7 us
  starting transfers between devices: 11.2 us -> 35.7 us
  local copies, waits for them, and re-layouts: 19.2 us -> 0.07 us
  matrix products: 17.8 us -> 0 us
  between operations: 15.8 us -> 0.8 us
  Pallas kernels: 0 us -> 14 us
  other arithmetic: 13.3 us -> 1.58 us
    all_to_all x2 -> x0, waiting for transfers between devices: 50.5 us -> none  [the longest x1 39.6 us: local(): lax.all_to_all(filled.reshape(n_ep, capacity, columns), 'ep', split_axis=...]
    ppermute x0 -> x27, starting transfers between devices: none -> 35.7 us  [swap(): lax.ppermute(x, axis, [(i, i ^ mask) for i in range(lax.axis_size(axis))])]
    ppermute x0 -> x27, waiting for transfers between devices: none -> 29.7 us  [swap(): lax.ppermute(x, axis, [(i, i ^ mask) for i in range(lax.axis_size(axis))])]
    reduce_scatter x2 -> x0, waiting for transfers between devices: 21.5 us -> none  [the longest x1 13.4 us: local(): lax.psum_scatter(partial_out.reshape(sources, slots, width).astype(jnp.bf...]
    dot_general x6 -> x0, matrix products: 17.8 us -> none  [the longest x1 3.9 us: local(): jnp.dot(attended, out_weight, preferred_element_type=jnp.float32)]
    pallas_call x0 -> x7, Pallas kernels: none -> 14 us  [run(): pl.pallas_call(body, out_shape=[pltpu.VMEM(s, d) for s, d in outs[:kept]]...]
    all_to_all x2 -> x0, starting transfers between devices: 10.9 us -> none  [the longest x1 6.26 us: local(): lax.all_to_all(filled.reshape(n_ep, capacity, columns), 'ep', split_axis=...]
    scatter x1 -> x0, local copies, waits for them, and re-layouts: 6.79 us -> none  [local(): jnp.zeros((n_ep * capacity, columns), jnp.bfloat16).at[target]]
  transfers between devices with their start and end apart: 6 -> 27, of which waited for: 4 -> 9; matrix products, arithmetic and copies ran while one was open for 28% -> 1% of each run, Pallas kernels for 0% -> 17%
where the time goes in v1:
time: 82 us; the launch traced here: 81.9 us
  starting transfers between devices  35.7 us (44%)
  waiting for transfers between devices  29.7 us (36%)
  Pallas kernels  14 us (17%)
  other arithmetic  1.58 us (2%)
    ppermute x27, starting transfers between devices, swap(): lax.ppermute(x, axis, [(i, i ^ mask) for i in range(lax.axis_size(axis))])  35.7 us
    ppermute x27, waiting for transfers between devices, swap(): lax.ppermute(x, axis, [(i, i ^ mask) for i in range(lax.axis_size(axis))])  29.7 us
    pallas_call x7, Pallas kernels, run(): pl.pallas_call(body, out_shape=[pltpu.VMEM(s, d) for s, d in outs[:kept]]...  14 us
  transfers between devices with their start and end apart: 27, of which 9 were waited for; matrix products, arithmetic and copies ran while one was open for 1% of the time, Pallas kernels for 17%

profile of v1, /device:TPU:0, one launch (start us, length us, event | category | flops | bytes accessed | tf_op | source)
XLA Modules:
  0.0 81.9 jit_solution(14856047952626112424)
XLA Ops:
  1.2 3.9 %shard_map.149 = (bf16[704,2048]{1,0:T(8,128)(2,1)S(1)}, bf16[704,2048]{1,0:T(8,128)(2,1)S(1)}, bf16[704,2048]{1,0:T(8,128)(2,1)S(1)}, bf16[128,512]{1,0:T(8,128...) custom-call(bf16[128,1024]{1,0:T(8,128)(2,1)} %refs_0_.1, ...), custom_call_target="tpu_custom_call" | custom-call | flops 7864320 | bytes 9175040 | tf_op jit(solution)/shard_map/pallas_call | solution.py:190
  5.1 2.6 %collective-permute-start = (bf16[256,512]{1,0:T(8,128)(2,1)S(1)}, bf16[256,512]{1,0:T(8,128)(2,1)S(1)}, u32[]{:S(2)}, u32[]{:S(2)}) collective-permute-start(bf16[256,512]{1,0:T(8,128)(2,1)S(1)} %get-tuple-element.32), channel_id=1, source_target_pairs={{0,8},{4,12},{8,0},{12,4},{16,24},{20,28},{24,16},{28,20},{1,9},{5... | collective-permute-start | bytes 786440 | tf_op jit(solution)/shard_map/ppermute | solution.py:174
  8.0 2.5 %collective-permute-start.2 = (bf16[128,512]{1,0:T(8,128)(2,1)S(1)}, bf16[128,512]{1,0:T(8,128)(2,1)S(1)}, u32[]{:S(2)}, u32[]{:S(2)}) collective-permute-start(bf16[128,512]{1,0:T(8,128)(2,1)S(1)} %get-tuple-element.34), channel_id=1, source_target_pairs={{0,24},{4,28},{8,16},{12,20},{16,8},{20,12},{24,0},{28,4},{1,25},{... | collective-permute-start | bytes 393224 | tf_op jit(solution)/shard_map/ppermute | solution.py:174
  10.6 1.8 %shard_map.152 = (bf16[80,2048]{1,0:T(8,128)(2,1)S(1)}, bf16[80,512]{1,0:T(8,128)(2,1)S(1)}, bf16[80,512]{1,0:T(8,128)(2,1)S(1)}, bf16[80,512]{1,0:T(8,128)(2,1)...) custom-call(bf16[128,2048]{1,0:T(8,128)(2,1)} %x0_hbm.1, f32[1,2048]{1,0:T(1,128)} %bitcast.21, ...), custom_call_target="tpu_custom_call" | custom-call | flops 335544320 | bytes 1048576 | tf_op jit(solution)/shard_map/pallas_call | solution.py:190
  12.4 1.9 %collective-permute-start.14 = (bf16[80,512]{1,0:T(8,128)(2,1)S(1)}, bf16[80,512]{1,0:T(8,128)(2,1)S(1)}, u32[]{:S(2)}, u32[]{:S(2)}) collective-permute-start(bf16[80,512]{1,0:T(8,128)(2,1)S(1)} %get-tuple-element.51), channel_id=1, source_target_pairs={{0,8},{4,12},{8,0},{12,4},{16,24},{20,28},{24,16},{28,20},{1,9},{5... | collective-permute-start | bytes 245768 | tf_op jit(solution)/shard_map/ppermute | solution.py:174
  14.2 5.6 %collective-permute-done = bf16[256,512]{1,0:T(8,128)(2,1)S(1)} collective-permute-done((bf16[256,512]{1,0:T(8,128)(2,1)S(1)}, bf16[256,512]{1,0:T(8,128)(2,1)S(1)}, u32[]{:S(2)}, u32[]{:S(2)}) %collective-permute-start) | collective-permute-done | bytes 262176 | tf_op jit(solution)/shard_map/ppermute | solution.py:174
  21.1 2.0 %collective-permute-start.16 = (bf16[80,512]{1,0:T(8,128)(2,1)S(1)}, bf16[80,512]{1,0:T(8,128)(2,1)S(1)}, u32[]{:S(2)}, u32[]{:S(2)}) collective-permute-start(bf16[80,512]{1,0:T(8,128)(2,1)S(1)} %get-tuple-element.53), channel_id=1, source_target_pairs={{0,24},{4,28},{8,16},{12,20},{16,8},{20,12},{24,0},{28,4},{1,25},{... | collective-permute-start | bytes 245768 | tf_op jit(solution)/shard_map/ppermute | solution.py:174
  23.1 6.2 %collective-permute-done.15 = bf16[80,512]{1,0:T(8,128)(2,1)S(1)} collective-permute-done((bf16[80,512]{1,0:T(8,128)(2,1)S(1)}, bf16[80,512]{1,0:T(8,128)(2,1)S(1)}, u32[]{:S(2)}, u32[]{:S(2)}) %collective-permute-start.15) | collective-permute-done | bytes 81952 | tf_op jit(solution)/shard_map/ppermute | solution.py:174
  29.3 1.7 %collective-permute-start.17 = (bf16[240,512]{1,0:T(8,128)(2,1)S(1)}, bf16[240,512]{1,0:T(8,128)(2,1)S(1)}, u32[]{:S(2)}, u32[]{:S(2)}) collective-permute-start(bf16[240,512]{1,0:T(8,128)(2,1)S(1)} %constant_dynamic-update-slice_fusion.refs_0_), channel_id=1, source_target_pairs={{0,1},{1,0},{2,3},{3,2},{4,5},{5,4},{6,7},{7,6},{8,9},{9,8},{10,11... | collective-permute-start | bytes 737288 | tf_op jit(solution)/shard_map/ppermute | solution.py:174
  31.0 1.5 %collective-permute-start.18 = (bf16[240,512]{1,0:T(8,128)(2,1)S(1)}, bf16[240,512]{1,0:T(8,128)(2,1)S(1)}, u32[]{:S(2)}, u32[]{:S(2)}) collective-permute-start(bf16[240,512]{1,0:T(8,128)(2,1)S(1)} %constant_dynamic-update-slice_fusion.refs_0_), channel_id=1, source_target_pairs={{0,2},{1,3},{2,0},{3,1},{4,6},{5,7},{6,4},{7,5},{8,10},{9,11},{10,... | collective-permute-start | bytes 737288 | tf_op jit(solution)/shard_map/ppermute | solution.py:174
  33.0 5.0 %collective-permute-done.17.refs_1_ = bf16[240,512]{1,0:T(8,128)(2,1)S(1)} collective-permute-done((bf16[240,512]{1,0:T(8,128)(2,1)S(1)}, bf16[240,512]{1,0:T(8,128)(2,1)S(1)}, u32[]{:S(2)}, u32[]{:S(2)}) %collective-permute-start.17) | collective-permute-done | bytes 245792 | tf_op jit(solution)/shard_map/ppermute | solution.py:174
  38.0 3.9 %collective-permute-done.18.refs_2_ = bf16[240,512]{1,0:T(8,128)(2,1)S(1)} collective-permute-done((bf16[240,512]{1,0:T(8,128)(2,1)S(1)}, bf16[240,512]{1,0:T(8,128)(2,1)S(1)}, u32[]{:S(2)}, u32[]{:S(2)}) %collective-permute-start.18) | collective-permute-done | bytes 245792 | tf_op jit(solution)/shard_map/ppermute | solution.py:174
  41.9 2.6 %shard_map.154 = (bf16[240,512]{1,0:T(8,128)(2,1)S(1)}, bf16[240,512]{1,0:T(8,128)(2,1)S(1)}, bf16[240,512]{1,0:T(8,128)(2,1)S(1)}, bf16[240,512]{1,0:T(8,128)(2,1)S(1)}) custom-call(bf16[240,512]{1,0:T(8,128)(2,1)S(1)} %constant_dynamic-update-slice_fusion.refs_0_, bf16[240,512]{1,0:T(8,128)(2,1)S(1)} %collective-permute-done.17.refs_1_, ...), custom_call_target="tpu_custom_call" | custom-call | flops 2076180480 | bytes 8650752 | tf_op jit(solution)/shard_map/pallas_call | solution.py:190
  44.4 1.5 %collective-permute-start.22 = (bf16[240,512]{1,0:T(8,128)(2,1)S(1)}, bf16[240,512]{1,0:T(8,128)(2,1)S(1)}, u32[]{:S(2)}, u32[]{:S(2)}) collective-permute-start(bf16[240,512]{1,0:T(8,128)(2,1)S(1)} %get-tuple-element.57), channel_id=1, source_target_pairs={{0,3},{1,2},{2,1},{3,0},{4,7},{5,6},{6,5},{7,4},{8,11},{9,10},{10,... | collective-permute-start | bytes 737288 | tf_op jit(solution)/shard_map/ppermute | solution.py:174
  48.0 2.4 %shard_map.153 = (bf16[80,512]{1,0:T(8,128)(2,1)S(1)}, bf16[80,512]{1,0:T(8,128)(2,1)S(1)}, bf16[80,512]{1,0:T(8,128)(2,1)S(1)}, bf16[80,512]{1,0:T(8,128)(2,1)S(1)}) custom-call(bf16[80,2048]{1,0:T(8,128)(2,1)S(1)} %get-tuple-element.43.refs_0_, bf16[704,2048]{1,0:T(8,128)(2,1)S(1)} %get-tuple-element.44.refs_1_.refs_4_, ...), custom_call_target="tpu_custom_call" | custom-call | flops 692060160 | bytes 8650752 | tf_op jit(solution)/shard_map/pallas_call | solution.py:190
  51.6 2.1 %shard_map.150 = (bf16[128,512]{1,0:T(8,128)(2,1)S(1)}, bf16[128,512]{1,0:T(8,128)(2,1)S(1)}) custom-call(bf16[128,512]{1,0:T(8,128)(2,1)S(1)} %get-tuple-element.31.q0, bf16[128,512]{1,0:T(8,128)(2,1)S(1)} %get-tuple-element.61.q1, bf16[512,512]{1,0:T(8,128)(2,1)S(1)} %pad_maximum_fusion.own, bf16[512,512]{1,0:T(8,128)(2,1)S(1)} %collective-permute-done.3.other), custom_call_target="tpu_custom_call" | custom-call | flops 536870912 | bytes 4194304 | tf_op jit(solution)/shard_map/pallas_call | solution.py:190
  56.5 3.4 %collective-permute-start.4 = (bf16[128,512]{1,0:T(8,128)(2,1)S(1)}, bf16[128,512]{1,0:T(8,128)(2,1)S(1)}, u32[]{:S(2)}, u32[]{:S(2)}) collective-permute-start(bf16[128,512]{1,0:T(8,128)(2,1)S(1)} %get-tuple-element.36), channel_id=1, source_target_pairs={{0,8},{4,12},{8,0},{12,4},{16,24},{20,28},{24,16},{28,20},{1,9},{5... | collective-permute-start | bytes 393224 | tf_op jit(solution)/shard_map/ppermute | solution.py:174
  60.1 2.8 %collective-permute-done.4.refs_1_ = bf16[128,512]{1,0:T(8,128)(2,1)S(1)} collective-permute-done((bf16[128,512]{1,0:T(8,128)(2,1)S(1)}, bf16[128,512]{1,0:T(8,128)(2,1)S(1)}, u32[]{:S(2)}, u32[]{:S(2)}) %collective-permute-start.4) | collective-permute-done | bytes 131104 | tf_op jit(solution)/shard_map/ppermute | solution.py:174
  62.9 2.0 %collective-permute-start.23 = (bf16[80,512]{1,0:T(8,128)(2,1)S(1)}, bf16[80,512]{1,0:T(8,128)(2,1)S(1)}, u32[]{:S(2)}, u32[]{:S(2)}) collective-permute-start(bf16[80,512]{1,0:T(8,128)(2,1)S(1)} %get-tuple-element.64), channel_id=1, source_target_pairs={{0,8},{4,12},{8,0},{12,4},{16,24},{20,28},{24,16},{28,20},{1,9},{5... | collective-permute-start | bytes 245768 | tf_op jit(solution)/shard_map/ppermute | solution.py:174
  65.7 1.6 %collective-permute-start.7 = (bf16[32,2048]{1,0:T(8,128)(2,1)S(1)}, bf16[32,2048]{1,0:T(8,128)(2,1)S(1)}, u32[]{:S(2)}, u32[]{:S(2)}) collective-permute-start(bf16[32,2048]{1,0:T(8,128)(2,1)S(1)} %get-tuple-element.40), channel_id=1, source_target_pairs={{0,3},{1,2},{2,1},{3,0},{4,7},{5,6},{6,5},{7,4},{8,11},{9,10},{10,... | collective-permute-start | bytes 393224 | tf_op jit(solution)/shard_map/ppermute | solution.py:174
  67.3 1.5 %collective-permute-start.6 = (bf16[32,2048]{1,0:T(8,128)(2,1)S(1)}, bf16[32,2048]{1,0:T(8,128)(2,1)S(1)}, u32[]{:S(2)}, u32[]{:S(2)}) collective-permute-start(bf16[32,2048]{1,0:T(8,128)(2,1)S(1)} %get-tuple-element.39), channel_id=1, source_target_pairs={{0,2},{1,3},{2,0},{3,1},{4,6},{5,7},{6,4},{7,5},{8,10},{9,11},{10,... | collective-permute-start | bytes 393224 | tf_op jit(solution)/shard_map/ppermute | solution.py:174
  69.3 3.5 %collective-permute-start.24 = (bf16[80,512]{1,0:T(8,128)(2,1)S(1)}, bf16[80,512]{1,0:T(8,128)(2,1)S(1)}, u32[]{:S(2)}, u32[]{:S(2)}) collective-permute-start(bf16[80,512]{1,0:T(8,128)(2,1)S(1)} %get-tuple-element.63), channel_id=1, source_target_pairs={{0,16},{4,20},{8,24},{12,28},{16,0},{20,4},{24,8},{28,12},{1,17},{... | collective-permute-start | bytes 245768 | tf_op jit(solution)/shard_map/ppermute | solution.py:174
  74.0 3.4 %collective-permute-done.24.refs_5_ = bf16[80,512]{1,0:T(8,128)(2,1)S(1)} collective-permute-done((bf16[80,512]{1,0:T(8,128)(2,1)S(1)}, bf16[80,512]{1,0:T(8,128)(2,1)S(1)}, u32[]{:S(2)}, u32[]{:S(2)}) %collective-permute-start.24) | collective-permute-done | bytes 81952 | tf_op jit(solution)/shard_map/ppermute | solution.py:174
  77.4 1.7 %collective-permute-done.25.refs_6_ = bf16[80,512]{1,0:T(8,128)(2,1)S(1)} collective-permute-done((bf16[80,512]{1,0:T(8,128)(2,1)S(1)}, bf16[80,512]{1,0:T(8,128)(2,1)S(1)}, u32[]{:S(2)}, u32[]{:S(2)}) %collective-permute-start.25) | collective-permute-done | bytes 81952 | tf_op jit(solution)/shard_map/ppermute | solution.py:174
  (52 shorter events, 14.2 us)
Async XLA Ops:
  0.6 9.9 %collective-permute-start.9 = (bf16[128,2048]{1,0:T(8,128)(2,1)}, bf16[128,2048]{1,0:T(8,128)(2,1)S(1)}, u32[]{:S(2)}, u32[]{:S(2)}) collective-permute-start(bf16[128,2048]{1,0:T(8,128)(2,1)} %x0_hbm.1), channel_id=1, source_target_pairs={{0,4},{4,0},{8,12},{12,8},{16,20},{20,16},{24,28},{28,24},{1,5},{5... | collective-permute-start | bytes 1572872 | tf_op jit(solution)/shard_map/ppermute | solution.py:174
  5.1 14.7 %collective-permute-start = (bf16[256,512]{1,0:T(8,128)(2,1)S(1)}, bf16[256,512]{1,0:T(8,128)(2,1)S(1)}, u32[]{:S(2)}, u32[]{:S(2)}) collective-permute-start(bf16[256,512]{1,0:T(8,128)(2,1)S(1)} %get-tuple-element.32), channel_id=1, source_target_pairs={{0,8},{4,12},{8,0},{12,4},{16,24},{20,28},{24,16},{28,20},{1,9},{5... | collective-permute-start | bytes 786440 | tf_op jit(solution)/shard_map/ppermute | solution.py:174
  8.0 24.9 %collective-permute-start.2 = (bf16[128,512]{1,0:T(8,128)(2,1)S(1)}, bf16[128,512]{1,0:T(8,128)(2,1)S(1)}, u32[]{:S(2)}, u32[]{:S(2)}) collective-permute-start(bf16[128,512]{1,0:T(8,128)(2,1)S(1)} %get-tuple-element.34), channel_id=1, source_target_pairs={{0,24},{4,28},{8,16},{12,20},{16,8},{20,12},{24,0},{28,4},{1,25},{... | collective-permute-start | bytes 393224 | tf_op jit(solution)/shard_map/ppermute | solution.py:174
  10.4 22.5 %collective-permute-start.1 = (bf16[128,512]{1,0:T(8,128)(2,1)S(1)}, bf16[128,512]{1,0:T(8,128)(2,1)S(1)}, u32[]{:S(2)}, u32[]{:S(2)}) collective-permute-start(bf16[128,512]{1,0:T(8,128)(2,1)S(1)} %get-tuple-element.33), channel_id=1, source_target_pairs={{0,16},{4,20},{8,24},{12,28},{16,0},{20,4},{24,8},{28,12},{1,17},{... | collective-permute-start | bytes 393224 | tf_op jit(solution)/shard_map/ppermute | solution.py:174
  12.4 10.7 %collective-permute-start.14 = (bf16[80,512]{1,0:T(8,128)(2,1)S(1)}, bf16[80,512]{1,0:T(8,128)(2,1)S(1)}, u32[]{:S(2)}, u32[]{:S(2)}) collective-permute-start(bf16[80,512]{1,0:T(8,128)(2,1)S(1)} %get-tuple-element.51), channel_id=1, source_target_pairs={{0,8},{4,12},{8,0},{12,4},{16,24},{20,28},{24,16},{28,20},{1,9},{5... | collective-permute-start | bytes 245768 | tf_op jit(solution)/shard_map/ppermute | solution.py:174
  19.8 9.5 %collective-permute-start.15 = (bf16[80,512]{1,0:T(8,128)(2,1)S(1)}, bf16[80,512]{1,0:T(8,128)(2,1)S(1)}, u32[]{:S(2)}, u32[]{:S(2)}) collective-permute-start(bf16[80,512]{1,0:T(8,128)(2,1)S(1)} %get-tuple-element.52), channel_id=1, source_target_pairs={{0,16},{4,20},{8,24},{12,28},{16,0},{20,4},{24,8},{28,12},{1,17},{... | collective-permute-start | bytes 245768 | tf_op jit(solution)/shard_map/ppermute | solution.py:174
  21.1 8.2 %collective-permute-start.16 = (bf16[80,512]{1,0:T(8,128)(2,1)S(1)}, bf16[80,512]{1,0:T(8,128)(2,1)S(1)}, u32[]{:S(2)}, u32[]{:S(2)}) collective-permute-start(bf16[80,512]{1,0:T(8,128)(2,1)S(1)} %get-tuple-element.53), channel_id=1, source_target_pairs={{0,24},{4,28},{8,16},{12,20},{16,8},{20,12},{24,0},{28,4},{1,25},{... | collective-permute-start | bytes 245768 | tf_op jit(solution)/shard_map/ppermute | solution.py:174
  29.3 8.7 %collective-permute-start.17 = (bf16[240,512]{1,0:T(8,128)(2,1)S(1)}, bf16[240,512]{1,0:T(8,128)(2,1)S(1)}, u32[]{:S(2)}, u32[]{:S(2)}) collective-permute-start(bf16[240,512]{1,0:T(8,128)(2,1)S(1)} %constant_dynamic-update-slice_fusion.refs_0_), channel_id=1, source_target_pairs={{0,1},{1,0},{2,3},{3,2},{4,5},{5,4},{6,7},{7,6},{8,9},{9,8},{10,11... | collective-permute-start | bytes 737288 | tf_op jit(solution)/shard_map/ppermute | solution.py:174
  31.0 10.8 %collective-permute-start.18 = (bf16[240,512]{1,0:T(8,128)(2,1)S(1)}, bf16[240,512]{1,0:T(8,128)(2,1)S(1)}, u32[]{:S(2)}, u32[]{:S(2)}) collective-permute-start(bf16[240,512]{1,0:T(8,128)(2,1)S(1)} %constant_dynamic-update-slice_fusion.refs_0_), channel_id=1, source_target_pairs={{0,2},{1,3},{2,0},{3,1},{4,6},{5,7},{6,4},{7,5},{8,10},{9,11},{10,... | collective-permute-start | bytes 737288 | tf_op jit(solution)/shard_map/ppermute | solution.py:174
  32.5 9.3 %collective-permute-start.19 = (bf16[240,512]{1,0:T(8,128)(2,1)S(1)}, bf16[240,512]{1,0:T(8,128)(2,1)S(1)}, u32[]{:S(2)}, u32[]{:S(2)}) collective-permute-start(bf16[240,512]{1,0:T(8,128)(2,1)S(1)} %constant_dynamic-update-slice_fusion.refs_0_), channel_id=1, source_target_pairs={{0,3},{1,2},{2,1},{3,0},{4,7},{5,6},{6,5},{7,4},{8,11},{9,10},{10,... | collective-permute-start | bytes 737288 | tf_op jit(solution)/shard_map/ppermute | solution.py:174
  32.9 17.4 %collective-permute-start.3 = (bf16[512,512]{1,0:T(8,128)(2,1)S(1)}, bf16[512,512]{1,0:T(8,128)(2,1)S(1)}, u32[]{:S(2)}, u32[]{:S(2)}) collective-permute-start(bf16[512,512]{1,0:T(8,128)(2,1)S(1)} %pad_maximum_fusion.own), channel_id=1, source_target_pairs={{0,4},{4,0},{8,12},{12,8},{16,20},{20,16},{24,28},{28,24},{1,5},{5... | collective-permute-start | bytes 1572872 | tf_op jit(solution)/shard_map/ppermute | solution.py:174
  44.4 9.3 %collective-permute-start.22 = (bf16[240,512]{1,0:T(8,128)(2,1)S(1)}, bf16[240,512]{1,0:T(8,128)(2,1)S(1)}, u32[]{:S(2)}, u32[]{:S(2)}) collective-permute-start(bf16[240,512]{1,0:T(8,128)(2,1)S(1)} %get-tuple-element.57), channel_id=1, source_target_pairs={{0,3},{1,2},{2,1},{3,0},{4,7},{5,6},{6,5},{7,4},{8,11},{9,10},{10,... | collective-permute-start | bytes 737288 | tf_op jit(solution)/shard_map/ppermute | solution.py:174
  46.0 9.1 %collective-permute-start.21 = (bf16[240,512]{1,0:T(8,128)(2,1)S(1)}, bf16[240,512]{1,0:T(8,128)(2,1)S(1)}, u32[]{:S(2)}, u32[]{:S(2)}) collective-permute-start(bf16[240,512]{1,0:T(8,128)(2,1)S(1)} %get-tuple-element.56), channel_id=1, source_target_pairs={{0,2},{1,3},{2,0},{3,1},{4,6},{5,7},{6,4},{7,5},{8,10},{9,11},{10,... | collective-permute-start | bytes 737288 | tf_op jit(solution)/shard_map/ppermute | solution.py:174
  47.2 9.3 %collective-permute-start.20 = (bf16[240,512]{1,0:T(8,128)(2,1)S(1)}, bf16[240,512]{1,0:T(8,128)(2,1)S(1)}, u32[]{:S(2)}, u32[]{:S(2)}) collective-permute-start(bf16[240,512]{1,0:T(8,128)(2,1)S(1)} %get-tuple-element.55), channel_id=1, source_target_pairs={{0,1},{1,0},{2,3},{3,2},{4,5},{5,4},{6,7},{7,6},{8,9},{9,8},{10,11... | collective-permute-start | bytes 737288 | tf_op jit(solution)/shard_map/ppermute | solution.py:174
  48.0 17.7 %collective-permute-start.8 = (f32[2,128]{1,0:T(2,128)S(1)}, f32[2,128]{1,0:T(2,128)S(1)}, u32[]{:S(2)}, u32[]{:S(2)}) collective-permute-start(f32[2,128]{1,0:T(2,128)S(1)} %bitcast.12), channel_id=1, source_target_pairs={{0,4},{4,0},{8,12},{12,8},{16,20},{20,16},{24,28},{28,24},{1,5},{5... | collective-permute-start | bytes 3080 | tf_op jit(solution)/shard_map/ppermute | solution.py:174
  50.4 16.9 %collective-permute-start.11 = (bf16[80,512]{1,0:T(8,128)(2,1)S(1)}, bf16[80,512]{1,0:T(8,128)(2,1)S(1)}, u32[]{:S(2)}, u32[]{:S(2)}) collective-permute-start(bf16[80,512]{1,0:T(8,128)(2,1)S(1)} %get-tuple-element.48), channel_id=1, source_target_pairs={{0,1},{1,0},{2,3},{3,2},{4,5},{5,4},{6,7},{7,6},{8,9},{9,8},{10,11... | collective-permute-start | bytes 245768 | tf_op jit(solution)/shard_map/ppermute | solution.py:174
  53.7 15.0 %collective-permute-start.12 = (bf16[80,512]{1,0:T(8,128)(2,1)S(1)}, bf16[80,512]{1,0:T(8,128)(2,1)S(1)}, u32[]{:S(2)}, u32[]{:S(2)}) collective-permute-start(bf16[80,512]{1,0:T(8,128)(2,1)S(1)} %get-tuple-element.49), channel_id=1, source_target_pairs={{0,2},{1,3},{2,0},{3,1},{4,6},{5,7},{6,4},{7,5},{8,10},{9,11},{10,... | collective-permute-start | bytes 245768 | tf_op jit(solution)/shard_map/ppermute | solution.py:174
  55.1 14.2 %collective-permute-start.13 = (bf16[80,512]{1,0:T(8,128)(2,1)S(1)}, bf16[80,512]{1,0:T(8,128)(2,1)S(1)}, u32[]{:S(2)}, u32[]{:S(2)}) collective-permute-start(bf16[80,512]{1,0:T(8,128)(2,1)S(1)} %get-tuple-element.50), channel_id=1, source_target_pairs={{0,3},{1,2},{2,1},{3,0},{4,7},{5,6},{6,5},{7,4},{8,11},{9,10},{10,... | collective-permute-start | bytes 245768 | tf_op jit(solution)/shard_map/ppermute | solution.py:174
  56.5 6.4 %collective-permute-start.4 = (bf16[128,512]{1,0:T(8,128)(2,1)S(1)}, bf16[128,512]{1,0:T(8,128)(2,1)S(1)}, u32[]{:S(2)}, u32[]{:S(2)}) collective-permute-start(bf16[128,512]{1,0:T(8,128)(2,1)S(1)} %get-tuple-element.36), channel_id=1, source_target_pairs={{0,8},{4,12},{8,0},{12,4},{16,24},{20,28},{24,16},{28,20},{1,9},{5... | collective-permute-start | bytes 393224 | tf_op jit(solution)/shard_map/ppermute | solution.py:174
  62.9 9.8 %collective-permute-start.23 = (bf16[80,512]{1,0:T(8,128)(2,1)S(1)}, bf16[80,512]{1,0:T(8,128)(2,1)S(1)}, u32[]{:S(2)}, u32[]{:S(2)}) collective-permute-start(bf16[80,512]{1,0:T(8,128)(2,1)S(1)} %get-tuple-element.64), channel_id=1, source_target_pairs={{0,8},{4,12},{8,0},{12,4},{16,24},{20,28},{24,16},{28,20},{1,9},{5... | collective-permute-start | bytes 245768 | tf_op jit(solution)/shard_map/ppermute | solution.py:174
  65.7 13.9 %collective-permute-start.7 = (bf16[32,2048]{1,0:T(8,128)(2,1)S(1)}, bf16[32,2048]{1,0:T(8,128)(2,1)S(1)}, u32[]{:S(2)}, u32[]{:S(2)}) collective-permute-start(bf16[32,2048]{1,0:T(8,128)(2,1)S(1)} %get-tuple-element.40), channel_id=1, source_target_pairs={{0,3},{1,2},{2,1},{3,0},{4,7},{5,6},{6,5},{7,4},{8,11},{9,10},{10,... | collective-permute-start | bytes 393224 | tf_op jit(solution)/shard_map/ppermute | solution.py:174
  67.3 12.4 %collective-permute-start.6 = (bf16[32,2048]{1,0:T(8,128)(2,1)S(1)}, bf16[32,2048]{1,0:T(8,128)(2,1)S(1)}, u32[]{:S(2)}, u32[]{:S(2)}) collective-permute-start(bf16[32,2048]{1,0:T(8,128)(2,1)S(1)} %get-tuple-element.39), channel_id=1, source_target_pairs={{0,2},{1,3},{2,0},{3,1},{4,6},{5,7},{6,4},{7,5},{8,10},{9,11},{10,... | collective-permute-start | bytes 393224 | tf_op jit(solution)/shard_map/ppermute | solution.py:174
  68.8 10.9 %collective-permute-start.5 = (bf16[32,2048]{1,0:T(8,128)(2,1)S(1)}, bf16[32,2048]{1,0:T(8,128)(2,1)S(1)}, u32[]{:S(2)}, u32[]{:S(2)}) collective-permute-start(bf16[32,2048]{1,0:T(8,128)(2,1)S(1)} %get-tuple-element.38), channel_id=1, source_target_pairs={{0,1},{1,0},{2,3},{3,2},{4,5},{5,4},{6,7},{7,6},{8,9},{9,8},{10,11... | collective-permute-start | bytes 393224 | tf_op jit(solution)/shard_map/ppermute | solution.py:174
  69.3 8.1 %collective-permute-start.24 = (bf16[80,512]{1,0:T(8,128)(2,1)S(1)}, bf16[80,512]{1,0:T(8,128)(2,1)S(1)}, u32[]{:S(2)}, u32[]{:S(2)}) collective-permute-start(bf16[80,512]{1,0:T(8,128)(2,1)S(1)} %get-tuple-element.63), channel_id=1, source_target_pairs={{0,16},{4,20},{8,24},{12,28},{16,0},{20,4},{24,8},{28,12},{1,17},{... | collective-permute-start | bytes 245768 | tf_op jit(solution)/shard_map/ppermute | solution.py:174
  (6 other events, 40.4 us)
